TPU v7x, 32 devices: a whole 2x2x4 slice. The times are simulated.
32 devices in a mesh: rep: 4 (over z), fs: 2 (over y), tp: 4 (over x, core).
Axes of the slice: x: 2, y: 2, z: 4, core: 2. Of those that a mesh axis runs over, the one named last changes fastest.
Arguments:
- tokens: bfloat16 [3072, 2048], P('rep', 'fs'), may hold values from -6 to 6
- gate_pre: bfloat16 [3072, 6144], P('rep', 'tp'), may hold values from -6 to 6
- up_pre: bfloat16 [3072, 6144], P('rep', 'tp'), may hold values from -6 to 6
- hidden_grad: bfloat16 [3072, 6144], P('rep', 'tp'), may hold values from -0.75 to 0.75
- gate_weight: bfloat16 [2048, 6144], P('fs', 'tp'), may hold values from -0.125 to 0.125
- up_weight: bfloat16 [2048, 6144], P('fs', 'tp'), may hold values from -0.125 to 0.125
- gate_taps: float32 [3, 6144], P(None, 'tp'), may hold values from -3.5 to 3.5
- up_taps: float32 [3, 6144], P(None, 'tp'), may hold values from -3.5 to 3.5
- gate_bias: float32 [6144], P('tp'), may hold values from -4 to 4
- up_bias: float32 [6144], P('tp'), may hold values from -4 to 4
Outputs:
- input_grad: bfloat16 [3072, 2048], P('rep', 'fs')
- gate_weight_grad: float32 [2048, 6144], P('fs', 'tp')
- up_weight_grad: float32 [2048, 6144], P('fs', 'tp')
- gate_taps_grad: float32 [3, 6144], P(None, 'tp')
- up_taps_grad: float32 [3, 6144], P(None, 'tp')
- gate_bias_grad: float32 [6144], P('tp')
- up_bias_grad: float32 [6144], P('tp')
All inputs are finite; a program needn't handle non-finite values.
Results may differ from a plain program's by a relative error of at most 0.017.
Values may be sent and summed in bfloat16 or wider, within the bound.
A program may use at most 64 MiB of HBM per device.

v0:
```python
import jax
import jax.numpy as jnp
from jax import lax
from jax.sharding import PartitionSpec as P


def causal_mix(signal, tap_weights):
    tap_count = tap_weights.shape[0]
    length = signal.shape[0]
    padded = jnp.pad(signal, ((tap_count - 1, 0), (0, 0)))
    mixed = padded[0:length] * tap_weights[0]
    for offset in range(1, tap_count):
        mixed = mixed + padded[offset : offset + length] * tap_weights[offset]
    return mixed


def mix_back(signal, tap_weights):
    tap_count = tap_weights.shape[0]
    length = signal.shape[0]
    padded = jnp.pad(signal, ((0, tap_count - 1), (0, 0)))
    begin = tap_count - 1
    mixed = padded[begin : begin + length] * tap_weights[0]
    for offset in range(1, tap_count):
        begin = tap_count - 1 - offset
        mixed = mixed + padded[begin : begin + length] * tap_weights[offset]
    return mixed


def tap_terms(grad_signal, signal, tap_count):
    length = signal.shape[0]
    padded = jnp.pad(signal, ((tap_count - 1, 0), (0, 0)))
    return jnp.stack(
        [
            jnp.sum(grad_signal * padded[offset : offset + length], axis=0)
            for offset in range(tap_count)
        ]
    )


def backward_terms(gate_pre, up_pre, hidden_grad, gate_taps, up_taps, gate_bias, up_bias):
    gate_float = gate_pre.astype(jnp.float32)
    up_float = up_pre.astype(jnp.float32)
    gate_mixed = causal_mix(gate_float, gate_taps) + gate_bias
    up_mixed = causal_mix(up_float, up_taps) + up_bias
    logistic = jax.nn.sigmoid(gate_mixed)
    cotangent = hidden_grad.astype(jnp.float32)
    gate_delta = cotangent * up_mixed * logistic * (1.0 + gate_mixed * (1.0 - logistic))
    up_delta = cotangent * gate_mixed * logistic
    gate_back = mix_back(gate_delta, gate_taps).astype(jnp.bfloat16)
    up_back = mix_back(up_delta, up_taps).astype(jnp.bfloat16)
    tap_count = gate_taps.shape[0]
    return (
        gate_back,
        up_back,
        tap_terms(gate_delta, gate_float, tap_count),
        tap_terms(up_delta, up_float, tap_count),
        jnp.sum(gate_delta, axis=0),
        jnp.sum(up_delta, axis=0),
    )


def per_device(
    tokens,
    gate_pre,
    up_pre,
    hidden_grad,
    gate_weight,
    up_weight,
    gate_taps,
    up_taps,
    gate_bias,
    up_bias,
):
    gate_back, up_back, gate_tap_part, up_tap_part, gate_bias_part, up_bias_part = backward_terms(
        gate_pre, up_pre, hidden_grad, gate_taps, up_taps, gate_bias, up_bias
    )
    feature_dims = (((1,), (1,)), ((), ()))
    token_dims = (((0,), (0,)), ((), ()))
    full_partial = lax.dot_general(
        gate_back, gate_weight, feature_dims, preferred_element_type=jnp.float32
    ) + lax.dot_general(up_back, up_weight, feature_dims, preferred_element_type=jnp.float32)
    own_columns = lax.psum_scatter(
        full_partial.astype(jnp.bfloat16), "tp", scatter_dimension=1, tiled=True
    )
    result = lax.all_gather(own_columns, "tp", axis=1, tiled=True)
    gate_local = lax.dot_general(tokens, gate_back, token_dims, preferred_element_type=jnp.float32)
    up_local = lax.dot_general(tokens, up_back, token_dims, preferred_element_type=jnp.float32)
    summed_grads = (
        lax.psum(gate_local.astype(jnp.bfloat16), "rep").astype(jnp.float32),
        lax.psum(up_local.astype(jnp.bfloat16), "rep").astype(jnp.float32),
        lax.psum(gate_tap_part.astype(jnp.bfloat16), "rep").astype(jnp.float32),
        lax.psum(up_tap_part.astype(jnp.bfloat16), "rep").astype(jnp.float32),
        lax.psum(gate_bias_part.astype(jnp.bfloat16), "rep").astype(jnp.float32),
        lax.psum(up_bias_part.astype(jnp.bfloat16), "rep").astype(jnp.float32),
    )
    gate_weight_grad, up_weight_grad, gate_taps_grad, up_taps_grad, gate_bias_grad, up_bias_grad = (
        summed_grads
    )
    return (
        result,
        gate_weight_grad,
        up_weight_grad,
        gate_taps_grad,
        up_taps_grad,
        gate_bias_grad,
        up_bias_grad,
    )


def solution(mesh):
    return jax.shard_map(
        per_device,
        mesh=mesh,
        in_specs=(
            P("rep", "fs"),
            P("rep", "tp"),
            P("rep", "tp"),
            P("rep", "tp"),
            P("fs", "tp"),
            P("fs", "tp"),
            P(None, "tp"),
            P(None, "tp"),
            P("tp"),
            P("tp"),
        ),
        out_specs=(
            P("rep", "fs"),
            P("fs", "tp"),
            P("fs", "tp"),
            P(None, "tp"),
            P(None, "tp"),
            P("tp"),
            P("tp"),
        ),
        check_vma=False,
    )
```

profile of v0, /device:TPU:0, one launch (start us, length us, event | category | flops | bytes accessed | tf_op | source)
XLA Modules:
  0.0 329.4 jit_solution(4718363927047613101)
XLA Ops:
  8.0 0.0 copy-start
  8.0 0.0 reduce-scatter.2.cloned.1.call-start
  8.1 1.0 slice_reduce_fusion.2
  9.1 1.0 slice_reduce_fusion.5
  10.0 2.3 convert_element_type.66
  12.4 0.0 copy-start.2
  12.4 0.6 convert_element_type.65
  13.0 1.0 copy-done.2
  14.0 5.8 %fusion.5 = (bf16[1536]{0:T(1024)(128)(2,1)S(1)}, bf16[1536]{0:T(1024)(128)(2,1)S(1)}, bf16[1536]{0:T(1024)(128)(2,1)S(1)}, bf16[1536]{0:T(1024)(128)(2,1)S(1)},...) fusion(bf16[768,1536]{1,0:T(8,128)(2,1)S(1)} %copy-done.3, f32[768,1536]{1,0:T(8,128)S(1)} %convert_element_type.65, ...), kind=kLoop, calls=%fused_computation.32 | loop fusion | flops 23586816 | bytes 23629824 | tf_op jit(solution)/shard_map/reduce_sum | solution.py:58
  19.8 10.3 %fusion.6 = (bf16[1536]{0:T(1024)(128)(2,1)S(1)}, bf16[1536]{0:T(1024)(128)(2,1)S(1)}, bf16[1536]{0:T(1024)(128)(2,1)S(1)}, bf16[1536]{0:T(1024)(128)(2,1)S(1)},...) fusion(bf16[768,1536]{1,0:T(8,128)(2,1)} %param.11, f32[768,1536]{1,0:T(8,128)S(1)} %convert_element_type.66, ...), kind=kLoop, calls=%fused_computation.33 | loop fusion | flops 35383296 | bytes 30707712 | tf_op jit(solution)/shard_map/reduce_sum | solution.py:57
  30.1 5.9 %add_convert_fusion.1 = bf16[768,1536]{1,0:T(8,128)(2,1)S(1)} fusion(f32[768,1536]{1,0:T(8,128)} %get-tuple-element.40, f32[1536]{0:T(1024)S(1)} %get-tuple-element.30, f32[1536]{0:T(1024)S(1)} %get-tuple-element.31, f32[1536]{0:T(1024)S(1)} %get-tuple-element.29), kind=kLoop, calls=%fused_computation.12 | loop fusion | flops 7077888 | bytes 7096320 | tf_op jit(solution)/shard_map/convert_element_type | solution.py:49
  36.1 2.6 fusion.9
  38.8 0.8 copy-done.9
  39.5 3.7 %add_convert_fusion.2 = bf16[768,1024]{1,0:T(8,128)(2,1)} fusion(f32[768,1024]{1,0:T(8,128)S(1)} %fusion.9, bf16[768,1536]{1,0:T(8,128)(2,1)S(1)} %copy-done.4, bf16[1024,1536]{1,0:T(8,128)(2,1)S(1)} %copy-done.9), kind=kOutput, calls=%fused_computation.23 | convolution fusion | flops 2417491968 | bytes 10223616 | tf_op jit(solution)/shard_map/dot_general | solution.py:81
  43.2 0.0 reduce-scatter.2.cloned.1.call-update
  43.3 0.0 all-gather.2.cloned.1.call-start
  43.3 30.9 %reduce-scatter.2.cloned.1.call-done = bf16[768,256]{1,0:T(8,128)(2,1)} async-done(((bf16[768,1024]{1,0:T(8,128)(2,1)}), bf16[768,256]{1,0:T(8,128)(2,1)}) %reduce-scatter.2.cloned.1.call-update) | async-done | bytes 393232 | tf_op jit(solution)/shard_map/reduce_scatter | solution.py:82
  74.2 0.0 all-gather.2.cloned.1.call-update
  74.2 0.0 all-reduce.8.cloned.1.call-start
  74.3 6.6 %fusion.3 = bf16[1024,1536]{0,1:T(8,128)(2,1)} fusion(bf16[768,1536]{1,0:T(8,128)(2,1)} %copy-done.6, bf16[768,1024]{1,0:T(8,128)(2,1)} %param.10), kind=kOutput, calls=%fused_computation.21 | convolution fusion | flops 2417491968 | bytes 7077888 | tf_op jit(solution)/shard_map/dot_general | solution.py:86
  80.9 4.0 %fusion.4 = bf16[1024,1536]{0,1:T(8,128)(2,1)} fusion(bf16[768,1536]{1,0:T(8,128)(2,1)S(1)} %copy-done.5, bf16[768,1024]{1,0:T(8,128)(2,1)S(1)} %copy-done.10), kind=kOutput, calls=%fused_computation.22 | convolution fusion | flops 2417491968 | bytes 7077888 | tf_op jit(solution)/shard_map/dot_general | solution.py:87
  84.9 0.0 all-reduce.8.cloned.1.call-update
  85.0 0.1 pad_maximum_fusion
  85.1 21.1 %all-reduce.4 = (bf16[3,1536]{1,0:T(4,128)(2,1)S(1)}, bf16[3,1536]{1,0:T(4,128)(2,1)S(1)}, bf16[1536]{0:T(1024)(128)(2,1)S(1)}, bf16[1536]{0:T(1024)(128)(2,1)S(1)}) all-reduce(bf16[3,1536]{1,0:T(4,128)(2,1)S(1)} %get-tuple-element.42, bf16[3,1536]{1,0:T(4,128)(2,1)S(1)} %get-tuple-element.43, ...), channel_id=1, replica_groups=mesh['rep'=4,'fs'=2,'tp'=4] {'rep'}, use_global_device_ids=true, to_apply=%region_6.7 | all-reduce | flops 12288 | bytes 49152 | tf_op jit(solution)/shard_map/psum | solution.py:91
  106.2 0.6 convert_element_type.79
  106.8 0.6 convert_element_type.81
  107.4 0.6 convert_element_type.76
  108.0 0.6 convert_element_type.77
  108.6 199.7 %all-reduce.8.cloned.1.call-done = (bf16[1024,1536]{0,1:T(8,128)(2,1)}, bf16[1024,1536]{0,1:T(8,128)(2,1)}) async-done(((bf16[1024,1536]{0,1:T(8,128)(2,1)}, bf16[1024,1536]{0,1:T(8,128)(2,1)}), (bf16[1024,1536]{0,1:T(8,128)(2,1)}, bf16[1024,1536]{0,1:T(8,128)(2,1)})) %all-reduce.8.cloned.1.call-update) | async-done | bytes 6291472 | tf_op jit(solution)/shard_map/psum | solution.py:89
  308.3 5.4 %copy.17 = f32[1024,1536]{1,0:T(8,128)} copy(bf16[1024,1536]{0,1:T(8,128)(2,1)} %get-tuple-element.36) | data formatting | bytes 9437184
  313.7 5.5 %copy.18 = f32[1024,1536]{1,0:T(8,128)} copy(bf16[1024,1536]{0,1:T(8,128)(2,1)} %get-tuple-element.37) | data formatting | bytes 9437184
  319.2 2.7 copy.22
  (25 shorter events, 0.1 us)
Async XLA Ops:
  8.0 28.1 %copy-start = (bf16[1024,1536]{1,0:T(8,128)(2,1)S(1)}, bf16[1024,1536]{1,0:T(8,128)(2,1)}, u32[]{:S(2)}) copy-start(bf16[1024,1536]{1,0:T(8,128)(2,1)} %param.14) | copy-start | bytes 9437188
  8.0 66.2 %reduce-scatter.2.cloned.1.call-start = ((), (), s32[]{:S(2)}) async-start(), calls=%async_computation.1 | async-start | bytes 1966080 | tf_op jit(solution)/shard_map/reduce_scatter | solution.py:82
  8.1 4.3 %copy-start.3 = (bf16[768,1536]{1,0:T(8,128)(2,1)S(1)}, bf16[768,1536]{1,0:T(8,128)(2,1)}, u32[]{:S(2)}) copy-start(bf16[768,1536]{1,0:T(8,128)(2,1)} %param.12) | copy-start | bytes 7077892
  12.4 1.7 copy-start.2
  12.4 1.7 copy-start.7
  14.0 5.8 %copy-start.8 = (f32[1536]{0:T(1024)S(1)}, f32[1536]{0:T(1024)}, u32[]{:S(2)}) copy-start(f32[1536]{0:T(1024)} %param.19) | copy-start | bytes 18436
  36.1 2.7 copy-start.6
  36.1 2.7 copy-start.4
  36.1 3.4 %copy-start.9 = (bf16[1024,1536]{1,0:T(8,128)(2,1)S(1)}, bf16[1024,1536]{1,0:T(8,128)(2,1)}, u32[]{:S(2)}) copy-start(bf16[1024,1536]{1,0:T(8,128)(2,1)} %param.15) | copy-start | bytes 9437188
  43.3 65.4 %all-gather.2.cloned.1.call-start = ((), (), s32[]{:S(2)}) async-start(), calls=%async_computation.2 | async-start | bytes 1966080 | tf_op jit(solution)/shard_map/all_gather | solution.py:85
  74.2 6.7 %copy-start.5 = (bf16[768,1536]{1,0:T(8,128)(2,1)S(1)}, bf16[768,1536]{1,0:T(8,128)(2,1)}, u32[]{:S(2)}) copy-start(bf16[768,1536]{1,0:T(8,128)(2,1)} %get-tuple-element.41) | copy-start | bytes 7077892
  74.2 234.1 %all-reduce.8.cloned.1.call-start = ((), (), s32[]{:S(2)}) async-start(), calls=%async_computation.3 | async-start | bytes 12582912 | tf_op jit(solution)/shard_map/psum | solution.py:89
  74.3 6.6 %copy-start.10 = (bf16[768,1024]{1,0:T(8,128)(2,1)S(1)}, bf16[768,1024]{1,0:T(8,128)(2,1)}, u32[]{:S(2)}) copy-start(bf16[768,1024]{1,0:T(8,128)(2,1)} %param.10) | copy-start | bytes 4718596
  313.7 8.2 %copy-start.1 = (bf16[1024,1536]{1,0:T(8,128)(2,1)S(1)}, bf16[1024,1536]{1,0:T(8,128)(2,1)}, u32[]{:S(2)}) copy-start(bf16[1024,1536]{1,0:T(8,128)(2,1)} %param.14) | copy-start | bytes 9437188
Sparse Core Ops, SparseCore 0:
  43.4 30.7 reduce-scatter.1
  75.7 19.8 all-gather.1
Sparse Core Ops, SparseCore 1:
  85.0 223.3 all-reduce.7
where the time goes:
time: 330 us; the launch traced here: 329 us
  waiting for transfers between devices  231 us (70%)
  other arithmetic  27.4 us (8%)
  blocking collectives  21.1 us (6%)
  local copies, waits for them, and re-layouts  17.4 us (5%)
  matrix products  17 us (5%)
  between operations  15.7 us (5%)
    psum x1, waiting for transfers between devices, per_device(): lax.psum(gate_local.astype(jnp.bfloat16), 'rep').astype(jnp.float32)  200 us
    reduce_scatter x1, waiting for transfers between devices, per_device(): lax.psum_scatter(full_partial.astype(jnp.bfloat16), 'tp', scatter_dimensi...  30.9 us
    psum x1, blocking collectives, per_device(): lax.psum(gate_tap_part.astype(jnp.bfloat16), 'rep').astype(jnp.float32)  21.1 us
    unnamed x25, local copies, waits for them, and re-layouts  15.4 us
    reduce_sum x1, other arithmetic, backward_terms(): jnp.sum(gate_delta, axis=0)  10.3 us
  transfers between devices with their start and end apart: 3, of which 2 were waited for; matrix products, arithmetic and copies ran while one was open for 4% of the time, Pallas kernels for 0%

commit v1 on v0

--- a/solution.py
+++ b/solution.py
@@ -86,7 +86,7 @@
     gate_local = lax.dot_general(tokens, gate_back, token_dims, preferred_element_type=jnp.float32)
     up_local = lax.dot_general(tokens, up_back, token_dims, preferred_element_type=jnp.float32)
     summed_grads = (
-        lax.psum(gate_local.astype(jnp.bfloat16), "rep").astype(jnp.float32),
+        lax.all_gather(gate_local.astype(jnp.bfloat16), "rep").sum(axis=0).astype(jnp.float32),
         lax.psum(up_local.astype(jnp.bfloat16), "rep").astype(jnp.float32),
         lax.psum(gate_tap_part.astype(jnp.bfloat16), "rep").astype(jnp.float32),
         lax.psum(up_tap_part.astype(jnp.bfloat16), "rep").astype(jnp.float32),

time: 330 us -> 427 us (1.29)
  waiting for transfers between devices: 231 us -> 288 us
  local copies, waits for them, and re-layouts: 17.4 us -> 36.6 us
  other arithmetic: 27.4 us -> 46.2 us
    psum x1, waiting for transfers between devices: 200 us -> 263 us  [per_device(): lax.psum(up_local.astype(jnp.bfloat16), 'rep').astype(jnp.float32)]
    all_gather x0 -> x1, local copies, waits for them, and re-layouts: none -> 21.2 us  [per_device(): lax.all_gather(gate_local.astype(jnp.bfloat16), 'rep').sum(axis=0)]
    reduce_sum x0 -> x1, other arithmetic: none -> 18.6 us  [per_device(): lax.all_gather(gate_local.astype(jnp.bfloat16), 'rep').sum(axis=0)]
    reduce_scatter x1, waiting for transfers between devices: 30.9 us -> 25.3 us  [per_device(): lax.psum_scatter(full_partial.astype(jnp.bfloat16), 'tp', scatter_dimensi...]
    unnamed x25 -> x27, local copies, waits for them, and re-layouts: 15.4 us -> 15.2 us
  transfers between devices with their start and end apart: 3 -> 4, of which waited for: 2 -> 2; matrix products, arithmetic and copies ran while one was open for 4% -> 5% of each run, Pallas kernels for 0% -> 0%
where the time goes in v1:
time: 427 us; the launch traced here: 426 us
  waiting for transfers between devices  288 us (67%)
  other arithmetic  46.2 us (11%)
  local copies, waits for them, and re-layouts  36.6 us (9%)
  blocking collectives  20.5 us (5%)
  matrix products  18.2 us (4%)
  between operations  15.4 us (4%)
    psum x1, waiting for transfers between devices, per_device(): lax.psum(up_local.astype(jnp.bfloat16), 'rep').astype(jnp.float32)  263 us
    reduce_scatter x1, waiting for transfers between devices, per_device(): lax.psum_scatter(full_partial.astype(jnp.bfloat16), 'tp', scatter_dimensi...  25.3 us
    all_gather x1, local copies, waits for them, and re-layouts, per_device(): lax.all_gather(gate_local.astype(jnp.bfloat16), 'rep').sum(axis=0)  21.2 us
    psum x1, blocking collectives, per_device(): lax.psum(gate_tap_part.astype(jnp.bfloat16), 'rep').astype(jnp.float32)  20.5 us
    reduce_sum x1, other arithmetic, per_device(): lax.all_gather(gate_local.astype(jnp.bfloat16), 'rep').sum(axis=0)  18.6 us
    unnamed x27, local copies, waits for them, and re-layouts  15.2 us
    reduce_sum x1, other arithmetic, backward_terms(): jnp.sum(gate_delta, axis=0)  10.3 us
  transfers between devices with their start and end apart: 4, of which 2 were waited for; matrix products, arithmetic and copies ran while one was open for 5% of the time, Pallas kernels for 0%

profile of v1, /device:TPU:0, one launch (start us, length us, event | category | flops | bytes accessed | tf_op | source)
XLA Modules:
  0.0 425.6 jit_solution(3481755478058599422)
XLA Ops:
  8.0 0.0 reduce-scatter.2.cloned.1.call-start
  8.1 2.5 convert_element_type.68
  10.5 0.0 copy-done.3
  10.6 0.6 convert_element_type.67
  11.2 0.1 copy-done.7
  11.3 0.1 slice_reduce_fusion.2
  11.4 0.1 slice_reduce_fusion.5
  11.4 0.8 copy-done.2
  12.3 5.8 %fusion.5 = (bf16[1536]{0:T(1024)(128)(2,1)S(1)}, bf16[1536]{0:T(1024)(128)(2,1)S(1)}, bf16[1536]{0:T(1024)(128)(2,1)S(1)}, bf16[1536]{0:T(1024)(128)(2,1)S(1)},...) fusion(bf16[768,1536]{1,0:T(8,128)(2,1)S(1)} %copy-done.3, f32[768,1536]{1,0:T(8,128)S(1)} %convert_element_type.67, ...), kind=kLoop, calls=%fused_computation.32 | loop fusion | flops 23586816 | bytes 23629824 | tf_op jit(solution)/shard_map/reduce_sum | solution.py:58
  18.1 10.3 %fusion.6 = (bf16[1536]{0:T(1024)(128)(2,1)S(1)}, bf16[1536]{0:T(1024)(128)(2,1)S(1)}, bf16[1536]{0:T(1024)(128)(2,1)S(1)}, bf16[1536]{0:T(1024)(128)(2,1)S(1)},...) fusion(bf16[768,1536]{1,0:T(8,128)(2,1)} %param.11, f32[768,1536]{1,0:T(8,128)S(1)} %convert_element_type.68, ...), kind=kLoop, calls=%fused_computation.33 | loop fusion | flops 35383296 | bytes 30707712 | tf_op jit(solution)/shard_map/reduce_sum | solution.py:57
  28.4 6.0 %add_convert_fusion.1 = bf16[768,1536]{1,0:T(8,128)(2,1)S(1)} fusion(f32[768,1536]{1,0:T(8,128)} %get-tuple-element.45, f32[1536]{0:T(1024)S(1)} %get-tuple-element.37, f32[1536]{0:T(1024)S(1)} %get-tuple-element.38, f32[1536]{0:T(1024)S(1)} %get-tuple-element.36), kind=kLoop, calls=%fused_computation.12 | loop fusion | flops 7077888 | bytes 7096320 | tf_op jit(solution)/shard_map/convert_element_type | solution.py:49
  34.4 2.6 fusion.9
  37.1 0.8 copy-done.11
  37.9 3.7 add_convert_fusion.2
  41.6 0.0 all-reduce.7.cloned.1.call-start
  41.7 5.5 %fusion.4 = bf16[1024,1536]{0,1:T(8,128)(2,1)} fusion(bf16[768,1536]{1,0:T(8,128)(2,1)S(1)} %copy-done.5, bf16[768,1024]{1,0:T(8,128)(2,1)} %param.10), kind=kOutput, calls=%fused_computation.22 | convolution fusion | flops 2417491968 | bytes 7077888 | tf_op jit(solution)/shard_map/dot_general | solution.py:87
  47.1 0.0 all-gather.4.cloned.1.call-start
  47.2 25.3 %reduce-scatter.2.cloned.1.call-done = bf16[768,256]{1,0:T(8,128)(2,1)} async-done(((bf16[768,1024]{1,0:T(8,128)(2,1)}), bf16[768,256]{1,0:T(8,128)(2,1)}) %reduce-scatter.2.cloned.1.call-update) | async-done | bytes 393232 | tf_op jit(solution)/shard_map/reduce_scatter | solution.py:82
  72.6 0.2 all-gather.6.cloned.1.call-start
  72.8 6.4 %fusion.3 = bf16[1024,1536]{0,1:T(8,128)(2,1)} fusion(bf16[768,1536]{1,0:T(8,128)(2,1)} %copy-done.6, bf16[768,1024]{1,0:T(8,128)(2,1)} %param.10), kind=kOutput, calls=%fused_computation.21 | convolution fusion | flops 2417491968 | bytes 7077888 | tf_op jit(solution)/shard_map/dot_general | solution.py:86
  79.3 0.1 pad_maximum_fusion
  79.4 20.5 %all-reduce.4 = (bf16[3,1536]{1,0:T(4,128)(2,1)S(1)}, bf16[3,1536]{1,0:T(4,128)(2,1)S(1)}, bf16[1536]{0:T(1024)(128)(2,1)S(1)}, bf16[1536]{0:T(1024)(128)(2,1)S(1)}) all-reduce(bf16[3,1536]{1,0:T(4,128)(2,1)S(1)} %get-tuple-element.47, bf16[3,1536]{1,0:T(4,128)(2,1)S(1)} %get-tuple-element.48, ...), channel_id=1, replica_groups=mesh['rep'=4,'fs'=2,'tp'=4] {'rep'}, use_global_device_ids=true, to_apply=%region_6.7 | all-reduce | flops 12288 | bytes 49152 | tf_op jit(solution)/shard_map/psum | solution.py:91
  99.9 0.6 convert_element_type.78
  100.5 0.6 convert_element_type.79
  101.1 0.6 convert_element_type.81
  101.7 0.6 convert_element_type.83
  102.3 262.8 %all-reduce.7.cloned.1.call-done = bf16[1024,1536]{0,1:T(8,128)(2,1)} async-done(((bf16[1024,1536]{0,1:T(8,128)(2,1)}), bf16[1024,1536]{0,1:T(8,128)(2,1)}) %all-reduce.7.cloned.1.call-update) | async-done | bytes 3145744 | tf_op jit(solution)/shard_map/psum | solution.py:90
  365.2 5.4 %copy.19 = f32[1024,1536]{1,0:T(8,128)} copy(bf16[1024,1536]{0,1:T(8,128)(2,1)} %all-reduce.7.cloned.1.call-done) | data formatting | bytes 9437184
  370.6 21.2 %reshape.16 = bf16[4,1024,1536]{1,0,2:T(4,128)(2,1)} reshape(bf16[4096,1536]{0,1:T(8,128)(2,1)} %all-gather.6.cloned.1.call-done) | data formatting | bytes 25165824 | tf_op jit(solution)/shard_map/all_gather | solution.py:89
  391.8 18.6 %reduce_sum.84 = bf16[1024,1536]{0,1:T(8,128)(2,1)} reduce(bf16[4,1024,1536]{1,0,2:T(4,128)(2,1)} %reshape.16, bf16[]{:T(256)} %constant.7.clone.1), dimensions={0}, to_apply=%region_1.2 | reduce | flops 4718592 | bytes 15728642 | tf_op jit(solution)/shard_map/reduce_sum | solution.py:89
  410.4 5.4 %copy.18 = f32[1024,1536]{1,0:T(8,128)} copy(bf16[1024,1536]{0,1:T(8,128)(2,1)} %reduce_sum.84) | data formatting | bytes 9437184
  415.8 2.7 copy.22
  (32 shorter events, 0.2 us)
Async XLA Ops:
  8.0 26.4 %copy-start = (bf16[1024,1536]{1,0:T(8,128)(2,1)S(1)}, bf16[1024,1536]{1,0:T(8,128)(2,1)}, u32[]{:S(2)}) copy-start(bf16[1024,1536]{1,0:T(8,128)(2,1)} %param.14) | copy-start | bytes 9437188
  8.0 64.5 %reduce-scatter.2.cloned.1.call-start = ((), (), s32[]{:S(2)}) async-start(), calls=%async_computation.1 | async-start | bytes 1966080 | tf_op jit(solution)/shard_map/reduce_scatter | solution.py:82
  8.1 2.5 copy-start.3
  10.6 0.7 copy-start.7
  10.6 0.8 copy-start.8
  10.6 1.7 copy-start.2
  10.6 1.7 copy-start.9
  12.3 5.8 %copy-start.10 = (f32[1536]{0:T(1024)S(1)}, f32[1536]{0:T(1024)}, u32[]{:S(2)}) copy-start(f32[1536]{0:T(1024)} %param.19) | copy-start | bytes 18436
  34.4 2.7 copy-start.6
  34.4 2.7 copy-start.4
  34.4 3.4 copy-start.11
  37.9 3.8 copy-start.5
  41.6 323.6 %all-reduce.7.cloned.1.call-start = ((), (), s32[]{:S(2)}) async-start(), calls=%async_computation.3 | async-start | bytes 6291456 | tf_op jit(solution)/shard_map/psum | solution.py:90
  47.1 323.4 %all-gather.4.cloned.1.call-start = ((), (), s32[]{:S(2)}) async-start(), calls=%async_computation.2 | async-start | bytes 1966080 | tf_op jit(solution)/shard_map/all_gather | solution.py:85
  72.6 298.0 %all-gather.6.cloned.1.call-start = ((), (), s32[]{:S(2)}) async-start(), calls=%async_computation.4 | async-start | bytes 15728640 | tf_op jit(solution)/shard_map/all_gather | solution.py:89
  391.8 26.6 %copy-start.1 = (bf16[1024,1536]{1,0:T(8,128)(2,1)S(1)}, bf16[1024,1536]{1,0:T(8,128)(2,1)}, u32[]{:S(2)}) copy-start(bf16[1024,1536]{1,0:T(8,128)(2,1)} %param.14) | copy-start | bytes 9437188
Sparse Core Ops, SparseCore 0:
  41.7 30.7 reduce-scatter.1
  74.1 19.8 all-gather.3
  96.1 252.3 all-gather.5
Sparse Core Ops, SparseCore 1:
  47.2 317.9 all-reduce.6
